TPU v7x, 32 devices: a whole 2x2x4 slice. The times are simulated.
32 devices in a mesh: fs: 8 (over z, y), tp: 4 (over x, core).
Axes of the slice: x: 2, y: 2, z: 4, core: 2. Of those that a mesh axis runs over, the one named last changes fastest.
Arguments:
- saved_input: bfloat16 [6144, 2048], P('fs'), may hold values from -6 to 6
- cot_inproj: bfloat16 [6144, 1024], P('fs', 'tp'), may hold values from -0.076171875 to 0.076171875
- cot_outproj: bfloat16 [6144, 1024], P('fs', 'tp'), may hold values from -0.076171875 to 0.076171875
- factor_inproj: bfloat16 [2048, 256], P('fs')
- factor_outproj: bfloat16 [2048, 256], P('fs')
- weight_inproj: float32 [2048, 1024], P('fs', 'tp'), may hold values from -0.125 to 0.125
- weight_outproj: float32 [2048, 1024], P('fs', 'tp'), may hold values from -0.125 to 0.125
- first_inproj: float32 [256, 1024], P('fs', 'tp'), may hold values from -6 to 6
- first_outproj: float32 [256, 1024], P('fs', 'tp'), may hold values from -6 to 6
- second_inproj: float32 [256, 1024], P('fs', 'tp'), may hold values from 0.25 to 4
- second_outproj: float32 [256, 1024], P('fs', 'tp'), may hold values from 0.25 to 4
Outputs:
- update_inproj: float32 [2048, 1024], P('fs', 'tp')
- update_outproj: float32 [2048, 1024], P('fs', 'tp')
- new_inproj: float32 [2048, 1024], P('fs', 'tp')
- new_outproj: float32 [2048, 1024], P('fs', 'tp')
- copy_inproj: bfloat16 [2048, 1024], P(None, 'tp')
- copy_outproj: bfloat16 [2048, 1024], P(None, 'tp')
- first_inproj_new: float32 [256, 1024], P('fs', 'tp')
- first_outproj_new: float32 [256, 1024], P('fs', 'tp')
- second_inproj_new: float32 [256, 1024], P('fs', 'tp')
- second_outproj_new: float32 [256, 1024], P('fs', 'tp')
All inputs are finite; a program needn't handle non-finite values.
Results may differ from a plain program's by a relative error of at most 0.00045.
Values may be sent and summed in bfloat16 or wider, within the bound.
No kernel may reach another device: no remote copies, remote signals or barrier semaphores. Data moves between devices by JAX's collectives and lax.ppermute only.
A program may use at most 64 MiB of HBM per device.

v0:
```python
import jax
import jax.numpy as jnp
from jax import lax
from jax.sharding import PartitionSpec as P


def contract_rows(left, right, precision):
    return lax.dot_general(
        left,
        right,
        (((0,), (0,)), ((), ())),
        precision=precision,
        preferred_element_type=jnp.float32,
    )


def on_device(
    saved_input,
    cot_inproj,
    cot_outproj,
    factor_inproj,
    factor_outproj,
    weight_inproj,
    weight_outproj,
    first_inproj,
    first_outproj,
    second_inproj,
    second_outproj,
):
    highest = lax.Precision.HIGHEST
    pieces = (
        lax.all_gather(factor_inproj, "fs", axis=0, tiled=True),
        lax.all_gather(factor_outproj, "fs", axis=0, tiled=True),
    )
    mapped_in = jnp.dot(saved_input, pieces[0], preferred_element_type=jnp.float32)
    mapped_out = jnp.dot(saved_input, pieces[1], preferred_element_type=jnp.float32)
    term_in = contract_rows(mapped_in, cot_inproj.astype(jnp.float32), highest)
    term_out = contract_rows(mapped_out, cot_outproj.astype(jnp.float32), highest)
    projected_in, projected_out = (
        lax.psum_scatter(term_in, "fs", scatter_dimension=0, tiled=True),
        lax.psum_scatter(term_out, "fs", scatter_dimension=0, tiled=True),
    )
    first_in_new = 0.8 * first_inproj + 0.2 * projected_in
    first_out_new = 0.8 * first_outproj + 0.2 * projected_out
    second_in_new = 0.9 * second_inproj + 0.1 * projected_in * projected_in
    second_out_new = 0.9 * second_outproj + 0.1 * projected_out * projected_out
    small_in = first_in_new / (jnp.sqrt(second_in_new) + 1e-08)
    small_out = first_out_new / (jnp.sqrt(second_out_new) + 1e-08)
    wide_in = factor_inproj.astype(jnp.float32)
    wide_out = factor_outproj.astype(jnp.float32)
    pieces = (
        lax.all_gather(small_in, "fs", axis=0, tiled=True),
        lax.all_gather(small_out, "fs", axis=0, tiled=True),
    )
    full_in = jnp.dot(wide_in, pieces[0], precision=highest)
    full_out = jnp.dot(wide_out, pieces[1], precision=highest)
    square_in, square_out = lax.psum(
        (jnp.sum(full_in * full_in), jnp.sum(full_out * full_out)), ("fs", "tp")
    )
    entries = float(full_in.shape[0] * full_in.shape[1] * lax.axis_size("fs") * lax.axis_size("tp"))
    update_in = full_in / jnp.sqrt(square_in / entries + 1e-06)
    update_out = full_out / jnp.sqrt(square_out / entries + 1e-06)
    fresh_in = weight_inproj - 0.02 * update_in
    fresh_out = weight_outproj - 0.02 * update_out
    copy_in, copy_out = (
        lax.all_gather(fresh_in.astype(jnp.bfloat16), "fs", axis=0, tiled=True),
        lax.all_gather(fresh_out.astype(jnp.bfloat16), "fs", axis=0, tiled=True),
    )
    return (
        update_in,
        update_out,
        fresh_in,
        fresh_out,
        copy_in,
        copy_out,
        first_in_new,
        first_out_new,
        second_in_new,
        second_out_new,
    )


def solution(mesh):
    return jax.shard_map(
        on_device,
        mesh=mesh,
        in_specs=(
            P("fs", None),
            P("fs", "tp"),
            P("fs", "tp"),
            P("fs", None),
            P("fs", None),
            P("fs", "tp"),
            P("fs", "tp"),
            P("fs", "tp"),
            P("fs", "tp"),
            P("fs", "tp"),
            P("fs", "tp"),
        ),
        out_specs=(
            P("fs", "tp"),
            P("fs", "tp"),
            P("fs", "tp"),
            P("fs", "tp"),
            P(None, "tp"),
            P(None, "tp"),
            P("fs", "tp"),
            P("fs", "tp"),
            P("fs", "tp"),
            P("fs", "tp"),
        ),
        check_vma=False,
    )
```

profile of v0, /device:TPU:0, one launch (start us, length us, event | category | flops | bytes accessed | tf_op | source)
XLA Modules:
  0.0 389.0 jit_solution(17355608462318028329)
XLA Ops:
  7.2 0.0 copy-start
  7.2 0.0 all-gather.5.cloned.1.call-start
  7.2 0.7 all-gather.5.cloned.1.call-update
  7.9 0.0 all-gather.7.cloned.1.call-start
  8.0 0.7 all-gather.7.cloned.1.call-update
  8.7 0.0 reduce-scatter.3.cloned.1.call-start
  8.7 1.1 copy.21
  9.8 43.4 %all-gather.5.cloned.1.call-done = bf16[2048,256]{1,0:T(8,128)(2,1)} async-done(((bf16[256,256]{1,0:T(8,128)(2,1)}), bf16[2048,256]{1,0:T(8,128)(2,1)}) %all-gather.5.cloned.1.call-update) | async-done | bytes 1048592 | tf_op jit(solution)/shard_map/all_gather | solution.py:32
  53.2 0.0 copy-done
  53.2 0.0 copy-start.2
  53.2 2.3 fusion.6
  55.4 0.0 copy-done.2
  55.4 1.5 fusion.7
  56.9 0.0 reduce-scatter.3.cloned.1.call-update
  57.0 0.0 copy-start.1
  57.0 0.0 reduce-scatter.5.cloned.1.call-start
  57.0 37.3 %all-gather.7.cloned.1.call-done = bf16[2048,256]{1,0:T(8,128)(2,1)} async-done(((bf16[256,256]{1,0:T(8,128)(2,1)}), bf16[2048,256]{1,0:T(8,128)(2,1)}) %all-gather.7.cloned.1.call-update) | async-done | bytes 1048592 | tf_op jit(solution)/shard_map/all_gather | solution.py:33
  94.3 0.0 copy-start.3
  94.3 2.3 fusion.8
  96.6 0.0 copy-done.3
  96.6 1.5 fusion.9
  98.1 0.0 reduce-scatter.5.cloned.1.call-update
  98.1 0.0 all-gather.9.cloned.1.call-start
  98.2 60.9 %reduce-scatter.3.cloned.1.call-done = f32[32,256]{1,0:T(8,128)} async-done(((f32[256,256]{1,0:T(8,128)}), f32[32,256]{1,0:T(8,128)}) %reduce-scatter.3.cloned.1.call-update) | async-done | bytes 32784 | tf_op jit(solution)/shard_map/reduce_scatter | solution.py:40
  159.0 1.4 add_divide_fusion.1
  160.5 30.9 %all_gather.19 = f32[256,256]{1,0:T(8,128)S(1)} all-gather(f32[32,256]{1,0:T(8,128)S(1)} %get-tuple-element.31), channel_id=1, replica_groups=mesh['fs'=8,'tp'=4] {'fs'}, dimensions={0}, use_global_device_ids=true | all-gather | bytes 294912 | tf_op jit(solution)/shard_map/all_gather | solution.py:52
  191.4 0.0 copy-done.1
  191.4 1.7 multiply_reduce_fusion.1
  193.1 30.8 %reduce-scatter.5.cloned.1.call-done = f32[32,256]{1,0:T(8,128)} async-done(((f32[256,256]{1,0:T(8,128)}), f32[32,256]{1,0:T(8,128)}) %reduce-scatter.5.cloned.1.call-update) | async-done | bytes 32784 | tf_op jit(solution)/shard_map/reduce_scatter | solution.py:41
  223.9 1.4 add_divide_fusion
  225.3 30.9 %all_gather.21 = f32[256,256]{1,0:T(8,128)S(1)} all-gather(f32[32,256]{1,0:T(8,128)S(1)} %get-tuple-element.28), channel_id=1, replica_groups=mesh['fs'=8,'tp'=4] {'fs'}, dimensions={0}, use_global_device_ids=true | all-gather | bytes 294912 | tf_op jit(solution)/shard_map/all_gather | solution.py:53
  256.2 2.6 multiply_reduce_fusion
  258.8 37.9 %all-reduce = (f32[]{:T(128)}, f32[]{:T(128)}) all-reduce(f32[]{:T(128)} %get-tuple-element.34, f32[]{:T(128)} %get-tuple-element.36), channel_id=1, replica_groups=mesh['fs'=8,'tp'=4] {'fs','tp'}, use_global_device_ids=true, to_apply=%region_2.0 | all-reduce | flops 2 | bytes 16 | tf_op jit(solution)/shard_map/psum | solution.py:57
  297.4 1.8 fusion.3
  299.3 0.0 all-gather.9.cloned.1.call-update
  299.3 0.0 all-gather.11.cloned.1.call-start
  299.3 1.8 copy.22
  301.8 1.8 fusion.2
  303.6 0.0 all-gather.11.cloned.1.call-update
  303.7 1.8 copy.25
  305.4 1.8 copy.23
  307.2 1.8 copy.26
  309.0 0.8 copy.24
  309.9 29.7 %all-gather.9.cloned.1.call-done = bf16[2048,256]{0,1:T(8,128)(2,1)} async-done(((bf16[256,256]{0,1:T(8,128)(2,1)}), bf16[2048,256]{0,1:T(8,128)(2,1)}) %all-gather.9.cloned.1.call-update) | async-done | bytes 1048592 | tf_op jit(solution)/shard_map/all_gather | solution.py:66
  339.6 2.3 copy.27
  341.8 38.1 %all-gather.11.cloned.1.call-done = bf16[2048,256]{0,1:T(8,128)(2,1)} async-done(((bf16[256,256]{0,1:T(8,128)(2,1)}), bf16[2048,256]{0,1:T(8,128)(2,1)}) %all-gather.11.cloned.1.call-update) | async-done | bytes 1048592 | tf_op jit(solution)/shard_map/all_gather | solution.py:67
  379.9 2.3 copy.28
Async XLA Ops:
  7.2 46.0 %copy-start = (bf16[768,2048]{1,0:T(8,128)(2,1)S(1)}, bf16[768,2048]{1,0:T(8,128)(2,1)}, u32[]{:S(2)}) copy-start(bf16[768,2048]{1,0:T(8,128)(2,1)} %param.11) | copy-start | bytes 9437188
  7.2 46.0 %all-gather.5.cloned.1.call-start = ((), (), s32[]{:S(2)}) async-start(), calls=%async_computation.2 | async-start | bytes 1179648 | tf_op jit(solution)/shard_map/all_gather | solution.py:32
  7.9 86.4 %all-gather.7.cloned.1.call-start = ((), (), s32[]{:S(2)}) async-start(), calls=%async_computation.4 | async-start | bytes 1179648 | tf_op jit(solution)/shard_map/all_gather | solution.py:33
  8.7 150.4 %reduce-scatter.3.cloned.1.call-start = ((), (), s32[]{:S(2)}) async-start(), calls=%async_computation.3 | async-start | bytes 294912 | tf_op jit(solution)/shard_map/reduce_scatter | solution.py:40
  53.2 2.3 copy-start.2
  57.0 134.4 %copy-start.1 = (bf16[256,256]{1,0:T(8,128)(2,1)S(1)}, bf16[256,256]{1,0:T(8,128)(2,1)}, u32[]{:S(2)}) copy-start(bf16[256,256]{1,0:T(8,128)(2,1)} %param.14) | copy-start | bytes 393220
  57.0 166.9 %reduce-scatter.5.cloned.1.call-start = ((), (), s32[]{:S(2)}) async-start(), calls=%async_computation.5 | async-start | bytes 294912 | tf_op jit(solution)/shard_map/reduce_scatter | solution.py:41
  94.3 2.3 copy-start.3
  98.1 241.5 %all-gather.9.cloned.1.call-start = ((), (), s32[]{:S(2)}) async-start(), calls=%async_computation.6 | async-start | bytes 1179648 | tf_op jit(solution)/shard_map/all_gather | solution.py:66
  299.3 80.6 %all-gather.11.cloned.1.call-start = ((), (), s32[]{:S(2)}) async-start(), calls=%async_computation.7 | async-start | bytes 1179648 | tf_op jit(solution)/shard_map/all_gather | solution.py:67
Sparse Core Ops, SparseCore 0:
  10.1 42.9 all-gather.4
  55.3 38.9 all-gather.6
  98.2 60.7 reduce-scatter.2
  162.8 61.0 reduce-scatter.4
  299.4 40.1 all-gather.8
  341.5 38.3 all-gather.10
where the time goes:
time: 390 us; the launch traced here: 389 us
  waiting for transfers between devices  242 us (62%)
  blocking collectives  99.7 us (26%)
  between operations  15.6 us (4%)
  local copies, waits for them, and re-layouts  13.6 us (3%)
  matrix products  11.8 us (3%)
  other arithmetic  6.5 us (2%)
    reduce_scatter x1, waiting for transfers between devices, on_device(): lax.psum_scatter(term_in, 'fs', scatter_dimension=0, tiled=True)  60.9 us
    all_gather x1, waiting for transfers between devices, on_device(): lax.all_gather(factor_inproj, 'fs', axis=0, tiled=True)  43.4 us
    all_gather x1, waiting for transfers between devices, on_device(): lax.all_gather(fresh_out.astype(jnp.bfloat16), 'fs', axis=0, tiled=True)  38.1 us
    psum x1, blocking collectives, on_device(): lax.psum((jnp.sum(full_in * full_in), jnp.sum(full_out * full_out)), ('fs...  37.9 us
    all_gather x1, waiting for transfers between devices, on_device(): lax.all_gather(factor_outproj, 'fs', axis=0, tiled=True)  37.3 us
    all_gather x1, blocking collectives, on_device(): lax.all_gather(small_in, 'fs', axis=0, tiled=True)  30.9 us
    all_gather x1, blocking collectives, on_device(): lax.all_gather(small_out, 'fs', axis=0, tiled=True)  30.9 us
    reduce_scatter x1, waiting for transfers between devices, on_device(): lax.psum_scatter(term_out, 'fs', scatter_dimension=0, tiled=True)  30.8 us
  transfers between devices with their start and end apart: 6, of which 6 were waited for; matrix products, arithmetic and copies ran while one was open for 6% of the time, Pallas kernels for 0%

commit v1 on v0

--- a/solution.py
+++ b/solution.py
@@ -2,6 +2,9 @@
 import jax.numpy as jnp
 from jax import lax
 from jax.sharding import PartitionSpec as P
+from jax.lax import psum
+
+cover_the_stops_all = lambda patch: psum(psum(patch, axis_name="tp"), "fs")
 
 
 def contract_rows(left, right, precision):
@@ -54,8 +57,8 @@
     )
     full_in = jnp.dot(wide_in, pieces[0], precision=highest)
     full_out = jnp.dot(wide_out, pieces[1], precision=highest)
-    square_in, square_out = lax.psum(
-        (jnp.sum(full_in * full_in), jnp.sum(full_out * full_out)), ("fs", "tp")
+    square_in, square_out = cover_the_stops_all(
+        (jnp.sum(full_in * full_in), jnp.sum(full_out * full_out))
     )
     entries = float(full_in.shape[0] * full_in.shape[1] * lax.axis_size("fs") * lax.axis_size("tp"))
     update_in = full_in / jnp.sqrt(square_in / entries + 1e-06)

time: 390 us -> 375 us (0.962)
  blocking collectives: 99.7 us -> 88.2 us
  waiting for transfers between devices: 242 us -> 238 us
    psum x1 -> x2, blocking collectives: 37.9 us -> 26.3 us  [cover_the_stops_all = lambda patch: psum(psum(patch, axis_name='tp'), 'fs')]
where the time goes in v1:
time: 375 us; the launch traced here: 374 us
  waiting for transfers between devices  238 us (63%)
  blocking collectives  88.2 us (24%)
  between operations  15.6 us (4%)
  local copies, waits for them, and re-layouts  13.6 us (4%)
  matrix products  11.8 us (3%)
  other arithmetic  6.5 us (2%)
    reduce_scatter x1, waiting for transfers between devices, on_device(): lax.psum_scatter(term_in, 'fs', scatter_dimension=0, tiled=True)  60.9 us
    all_gather x1, waiting for transfers between devices, on_device(): lax.all_gather(factor_inproj, 'fs', axis=0, tiled=True)  43.4 us
    all_gather x1, waiting for transfers between devices, on_device(): lax.all_gather(fresh_out.astype(jnp.bfloat16), 'fs', axis=0, tiled=True)  38.1 us
    all_gather x1, waiting for transfers between devices, on_device(): lax.all_gather(factor_outproj, 'fs', axis=0, tiled=True)  37.3 us
    all_gather x1, blocking collectives, on_device(): lax.all_gather(small_in, 'fs', axis=0, tiled=True)  30.9 us
    all_gather x1, blocking collectives, on_device(): lax.all_gather(small_out, 'fs', axis=0, tiled=True)  30.9 us
    reduce_scatter x1, waiting for transfers between devices, on_device(): lax.psum_scatter(term_out, 'fs', scatter_dimension=0, tiled=True)  30.8 us
    all_gather x1, waiting for transfers between devices, on_device(): lax.all_gather(fresh_in.astype(jnp.bfloat16), 'fs', axis=0, tiled=True)  26.5 us
  transfers between devices with their start and end apart: 6, of which 6 were waited for; matrix products, arithmetic and copies ran while one was open for 6% of the time, Pallas kernels for 0%

profile of v1, /device:TPU:0, one launch (start us, length us, event | category | flops | bytes accessed | tf_op | source)
XLA Modules:
  0.0 374.2 jit_solution(2279226285364084912)
XLA Ops:
  7.2 0.0 copy-start
  7.2 0.0 all-gather.5.cloned.1.call-start
  7.2 0.7 all-gather.5.cloned.1.call-update
  7.9 0.0 all-gather.7.cloned.1.call-start
  8.0 0.7 all-gather.7.cloned.1.call-update
  8.7 0.0 reduce-scatter.3.cloned.1.call-start
  8.7 1.1 copy.21
  9.8 43.4 %all-gather.5.cloned.1.call-done = bf16[2048,256]{1,0:T(8,128)(2,1)} async-done(((bf16[256,256]{1,0:T(8,128)(2,1)}), bf16[2048,256]{1,0:T(8,128)(2,1)}) %all-gather.5.cloned.1.call-update) | async-done | bytes 1048592 | tf_op jit(solution)/shard_map/all_gather | solution.py:35
  53.2 0.0 copy-done
  53.2 0.0 copy-start.2
  53.2 2.3 fusion.6
  55.4 0.0 copy-done.2
  55.4 1.5 fusion.7
  56.9 0.0 reduce-scatter.3.cloned.1.call-update
  57.0 0.0 copy-start.1
  57.0 0.0 reduce-scatter.5.cloned.1.call-start
  57.0 37.3 %all-gather.7.cloned.1.call-done = bf16[2048,256]{1,0:T(8,128)(2,1)} async-done(((bf16[256,256]{1,0:T(8,128)(2,1)}), bf16[2048,256]{1,0:T(8,128)(2,1)}) %all-gather.7.cloned.1.call-update) | async-done | bytes 1048592 | tf_op jit(solution)/shard_map/all_gather | solution.py:36
  94.3 0.0 copy-start.3
  94.3 2.3 fusion.8
  96.6 0.0 copy-done.3
  96.6 1.5 fusion.9
  98.1 0.0 reduce-scatter.5.cloned.1.call-update
  98.1 0.0 all-gather.9.cloned.1.call-start
  98.2 60.9 %reduce-scatter.3.cloned.1.call-done = f32[32,256]{1,0:T(8,128)} async-done(((f32[256,256]{1,0:T(8,128)}), f32[32,256]{1,0:T(8,128)}) %reduce-scatter.3.cloned.1.call-update) | async-done | bytes 32784 | tf_op jit(solution)/shard_map/reduce_scatter | solution.py:43
  159.0 1.4 add_divide_fusion.1
  160.5 30.9 %all_gather.19 = f32[256,256]{1,0:T(8,128)S(1)} all-gather(f32[32,256]{1,0:T(8,128)S(1)} %get-tuple-element.33), channel_id=1, replica_groups=mesh['fs'=8,'tp'=4] {'fs'}, dimensions={0}, use_global_device_ids=true | all-gather | bytes 294912 | tf_op jit(solution)/shard_map/all_gather | solution.py:55
  191.4 0.0 copy-done.1
  191.4 1.7 multiply_reduce_fusion.1
  193.1 30.8 %reduce-scatter.5.cloned.1.call-done = f32[32,256]{1,0:T(8,128)} async-done(((f32[256,256]{1,0:T(8,128)}), f32[32,256]{1,0:T(8,128)}) %reduce-scatter.5.cloned.1.call-update) | async-done | bytes 32784 | tf_op jit(solution)/shard_map/reduce_scatter | solution.py:44
  223.9 1.4 add_divide_fusion
  225.3 30.9 %all_gather.21 = f32[256,256]{1,0:T(8,128)S(1)} all-gather(f32[32,256]{1,0:T(8,128)S(1)} %get-tuple-element.30), channel_id=1, replica_groups=mesh['fs'=8,'tp'=4] {'fs'}, dimensions={0}, use_global_device_ids=true | all-gather | bytes 294912 | tf_op jit(solution)/shard_map/all_gather | solution.py:56
  256.2 2.6 multiply_reduce_fusion
  258.8 6.3 %all-reduce.1 = (f32[]{:T(128)}, f32[]{:T(128)}) all-reduce(f32[]{:T(128)} %get-tuple-element.36, f32[]{:T(128)} %get-tuple-element.38), channel_id=1, replica_groups=mesh['fs'=8,'tp'=4] {'tp'}, use_global_device_ids=true, to_apply=%region_2.0 | all-reduce | flops 2 | bytes 16 | tf_op jit(solution)/shard_map/psum | solution.py:7
  265.1 20.1 %all-reduce = (f32[]{:T(128)}, f32[]{:T(128)}) all-reduce(f32[]{:T(128)} %get-tuple-element.22, f32[]{:T(128)} %get-tuple-element.23), channel_id=1, replica_groups=mesh['fs'=8,'tp'=4] {'fs'}, use_global_device_ids=true, to_apply=%region_3.0 | all-reduce | flops 2 | bytes 16 | tf_op jit(solution)/shard_map/psum | solution.py:7
  285.9 1.8 fusion.3
  287.7 0.0 all-gather.9.cloned.1.call-update
  287.7 0.0 all-gather.11.cloned.1.call-start
  287.8 1.8 copy.22
  290.3 1.8 fusion.2
  292.1 0.0 all-gather.11.cloned.1.call-update
  292.1 1.8 copy.25
  293.9 1.8 copy.23
  295.7 1.8 copy.26
  297.5 0.8 copy.24
  298.3 26.5 %all-gather.9.cloned.1.call-done = bf16[2048,256]{0,1:T(8,128)(2,1)} async-done(((bf16[256,256]{0,1:T(8,128)(2,1)}), bf16[2048,256]{0,1:T(8,128)(2,1)}) %all-gather.9.cloned.1.call-update) | async-done | bytes 1048592 | tf_op jit(solution)/shard_map/all_gather | solution.py:69
  324.8 2.3 copy.27
  327.0 38.1 %all-gather.11.cloned.1.call-done = bf16[2048,256]{0,1:T(8,128)(2,1)} async-done(((bf16[256,256]{0,1:T(8,128)(2,1)}), bf16[2048,256]{0,1:T(8,128)(2,1)}) %all-gather.11.cloned.1.call-update) | async-done | bytes 1048592 | tf_op jit(solution)/shard_map/all_gather | solution.py:70
  365.1 2.3 copy.28
Async XLA Ops:
  7.2 46.0 %copy-start = (bf16[768,2048]{1,0:T(8,128)(2,1)S(1)}, bf16[768,2048]{1,0:T(8,128)(2,1)}, u32[]{:S(2)}) copy-start(bf16[768,2048]{1,0:T(8,128)(2,1)} %param.11) | copy-start | bytes 9437188
  7.2 46.0 %all-gather.5.cloned.1.call-start = ((), (), s32[]{:S(2)}) async-start(), calls=%async_computation.2 | async-start | bytes 1179648 | tf_op jit(solution)/shard_map/all_gather | solution.py:35
  7.9 86.4 %all-gather.7.cloned.1.call-start = ((), (), s32[]{:S(2)}) async-start(), calls=%async_computation.4 | async-start | bytes 1179648 | tf_op jit(solution)/shard_map/all_gather | solution.py:36
  8.7 150.4 %reduce-scatter.3.cloned.1.call-start = ((), (), s32[]{:S(2)}) async-start(), calls=%async_computation.3 | async-start | bytes 294912 | tf_op jit(solution)/shard_map/reduce_scatter | solution.py:43
  53.2 2.3 copy-start.2
  57.0 134.4 %copy-start.1 = (bf16[256,256]{1,0:T(8,128)(2,1)S(1)}, bf16[256,256]{1,0:T(8,128)(2,1)}, u32[]{:S(2)}) copy-start(bf16[256,256]{1,0:T(8,128)(2,1)} %param.14) | copy-start | bytes 393220
  57.0 166.9 %reduce-scatter.5.cloned.1.call-start = ((), (), s32[]{:S(2)}) async-start(), calls=%async_computation.5 | async-start | bytes 294912 | tf_op jit(solution)/shard_map/reduce_scatter | solution.py:44
  94.3 2.3 copy-start.3
  98.1 226.7 %all-gather.9.cloned.1.call-start = ((), (), s32[]{:S(2)}) async-start(), calls=%async_computation.6 | async-start | bytes 1179648 | tf_op jit(solution)/shard_map/all_gather | solution.py:69
  287.7 77.4 %all-gather.11.cloned.1.call-start = ((), (), s32[]{:S(2)}) async-start(), calls=%async_computation.7 | async-start | bytes 1179648 | tf_op jit(solution)/shard_map/all_gather | solution.py:70
Sparse Core Ops, SparseCore 0:
  10.1 42.9 all-gather.4
  55.3 38.9 all-gather.6
  98.2 60.7 reduce-scatter.2
  162.8 61.0 reduce-scatter.4
  287.9 36.8 all-gather.8
  326.7 38.3 all-gather.10
